TPU v7x, 512 devices: a 8x2x16 block of a 8x16x16 slice. The times are simulated.
512 devices in a mesh: grp: 2 (over y), fs: 16 (over z), tp: 16 (over x, core).
Axes of the slice: x: 8, y: 2, z: 16, core: 2. Of those that a mesh axis runs over, the one named last changes fastest.
The devices are a block of a 8x16x16 slice.
Arguments:
- tokens: bfloat16 [16384, 2048], P(('grp', 'fs')), parts along dimension 0, may hold values from -6 to 6
- pre_gain: float32 [2048], replicated, may hold values from 0.1 to 1.9
- gate_weight: float32 [2048, 5632], P('fs', 'tp'), may hold values from -0.125 to 0.125
- gate_scale: float32 [5632], P('tp'), may hold values from 0.5 to 2
- up_weight: float32 [2048, 5632], P('fs', 'tp'), may hold values from -0.125 to 0.125
- up_scale: float32 [5632], P('tp'), may hold values from 0.5 to 2
- down_weight: float32 [5632, 2048], P('tp', 'fs'), may hold values from -0.078125 to 0.078125
- down_scale: float32 [2048], replicated, may hold values from 0.3 to 3
- post_gain: float32 [2048], replicated, may hold values from 0.1 to 1.9
Outputs:
- mixed: bfloat16 [16384, 2048], P(('grp', 'fs')), parts along dimension 0
There are 2 independent parts, one for each index of `grp`. A program takes and returns all parts, laid end to end along the dimension named above; an argument that names none is the same for every part. Nothing has to cross between parts.
All inputs are finite; a program needn't handle non-finite values.
Results may differ from a plain program's by a relative error of at most 0.018.
Values may be sent and summed in bfloat16 or wider, within the bound.
No kernel may reach another device: no remote copies, remote signals or barrier semaphores. Data moves between devices by JAX's collectives and lax.ppermute only.
A program may use at most 64 MiB of HBM per device.

v0:
```python
import jax
import jax.numpy as jnp
from jax import lax
from jax.sharding import PartitionSpec as P

EPS = 1e-06


def side_by_side(arrays, axis, dim, along):
    ends, at = ([], 0)
    for a in arrays[:-1]:
        at += a.shape[along]
        ends.append(at)
    both = jnp.concatenate(arrays, axis=along)
    return tuple(jnp.split(lax.all_gather(both, axis, axis=dim, tiled=True), ends, axis=along))


def from_everyone(array, axis):
    copies = jnp.broadcast_to(array, (lax.axis_size(axis), *array.shape))
    return lax.all_to_all(copies, axis, split_axis=0, concat_axis=0, tiled=True)


def joined_along(parts, dim):
    lengths = list(parts.shape[1:])
    lengths[dim] *= parts.shape[0]
    return jnp.moveaxis(parts, 0, dim).reshape(lengths)


def collect(array, axis, dim):
    parts = from_everyone(array, axis)
    return joined_along(parts, dim)


def cut_along(array, dim, count):
    lengths = array.shape
    parts = array.reshape(*lengths[:dim], count, lengths[dim] // count, *lengths[dim + 1 :])
    return jnp.moveaxis(parts, dim, 0)


def sent_and_summed(array, axis, dim):
    count = lax.axis_size(axis)
    parts = lax.all_to_all(cut_along(array, dim, count), axis, 0, 0, tiled=True)
    return jnp.sum(parts.astype(jnp.float32), axis=0)


def finish(summed, down_scale, post_gain):
    branch = summed * down_scale
    return (
        branch * lax.rsqrt(jnp.mean(branch * branch, axis=-1, keepdims=True) + EPS) * post_gain
    ).astype(jnp.bfloat16)


def body(
    tokens,
    pre_gain,
    gate_weight,
    gate_scale,
    up_weight,
    up_scale,
    down_weight,
    down_scale,
    post_gain,
):
    rows = tokens.astype(jnp.float32)
    normed = (
        rows * lax.rsqrt(jnp.mean(rows * rows, axis=-1, keepdims=True) + EPS) * pre_gain
    ).astype(jnp.bfloat16)
    gate_low = gate_weight.astype(jnp.bfloat16)
    up_low = up_weight.astype(jnp.bfloat16)
    down_low = down_weight.astype(jnp.bfloat16)
    gate_full, up_full = side_by_side((gate_low, up_low), "fs", 0, 1)
    gate = jnp.dot(normed, gate_full, preferred_element_type=jnp.float32) * gate_scale
    up = jnp.dot(normed, up_full, preferred_element_type=jnp.float32) * up_scale
    hidden = (jax.nn.silu(gate) * up).astype(jnp.bfloat16)
    down_full = collect(down_low, "fs", 1)
    summed = sent_and_summed(
        jnp.dot(hidden, down_full, preferred_element_type=jnp.float32).astype(jnp.bfloat16), "tp", 0
    )
    scaled = finish(summed, down_scale, post_gain)
    return lax.all_gather(scaled, "tp", axis=0, tiled=True)


def solution(mesh):
    in_specs = (
        P(("grp", "fs"), None),
        P(),
        P("fs", "tp"),
        P("tp"),
        P("fs", "tp"),
        P("tp"),
        P("tp", "fs"),
        P(),
        P(),
    )
    out_specs = P(("grp", "fs"), None)
    return jax.shard_map(body, mesh=mesh, in_specs=in_specs, out_specs=out_specs, check_vma=False)
```

profile of v0, /device:TPU:65, one launch (start us, length us, event | category | flops | bytes accessed | tf_op | source)
XLA Modules:
  0.0 292.3 jit_solution(8846115028078084117)
XLA Ops:
  6.5 0.0 all-gather.3.cloned.1.call-start
  6.6 0.9 convert_element_type.29
  7.5 0.9 convert_element_type.30
  8.4 0.7 pad_maximum_fusion
  9.1 0.1 all-gather.3.cloned.1.call-update
  9.2 0.9 convert_element_type.32
  10.1 0.0 copy-start
  10.1 1.3 broadcast_in_dim.2
  11.4 0.0 copy-start.3
  11.4 0.0 copy-start.4
  11.4 44.4 %all-to-all-start = ((bf16[16,352,128]{2,1,0:T(8,128)(2,1)}), bf16[16,352,128]{2,1,0:T(8,128)(2,1)S(1)}, u32[]{:S(2)}, u32[]{:S(2)}) async-start(bf16[16,352,128]{2,1,0:T(8,128)(2,1)} %broadcast_in_dim.2), calls=%async_computation | async-start | bytes 2883584 | tf_op jit(solution)/shard_map/all_to_all | solution.py:20
  55.8 0.1 all-gather.5.cloned.1.call-start
  55.9 0.0 copy-done
  55.9 0.5 fusion
  56.4 111.5 %all-gather.3.cloned.1.call-done = bf16[2048,704]{0,1:T(8,128)(2,1)} async-done(((bf16[128,704]{0,1:T(8,128)(2,1)}), bf16[2048,704]{0,1:T(8,128)(2,1)}) %all-gather.3.cloned.1.call-update) | async-done | bytes 2883600 | tf_op jit(solution)/shard_map/all_gather | solution.py:15
  167.8 0.0 copy-done.3
  167.8 0.0 copy-done.4
  167.8 3.2 %fusion.9 = f32[512,352]{0,1:T(8,128)} fusion(bf16[2048,704]{0,1:T(8,128)(2,1)} %all-gather.3.cloned.1.call-done, bf16[512,2048]{1,0:T(8,128)(2,1)S(1)} %copy-done, f32[2048]{0:T(1024)S(1)} %copy-done.3, f32[512]{0:T(512)S(1)} %add_rsqrt_fusion, f32[352]{0:T(512)S(1)} %copy-done.4), kind=kOutput, calls=%fused_computation.13 | convolution fusion | flops 742572032 | bytes 4271488 | tf_op jit(solution)/shard_map/dot_general | solution.py:72
  171.1 0.0 all-to-all-done
  171.1 5.2 %convolution_convert_fusion = bf16[512,2048]{1,0:T(8,128)(2,1)} fusion(bf16[2048,704]{0,1:T(8,128)(2,1)} %all-gather.3.cloned.1.call-done, f32[512,352]{0,1:T(8,128)} %fusion.9, bf16[512,2048]{1,0:T(8,128)(2,1)S(1)} %copy-done, f32[2048]{0:T(1024)S(1)} %copy-done.3, f32[512]{0:T(512)S(1)} %add_rsqrt_fusion, f32[352]{0:T(512)} %param.14, ...), kind=kOutput, calls=%fused_computation.6 | convolution fusion | flops 1482899456 | bytes 7811072 | tf_op jit(solution)/shard_map/dot_general | solution.py:77
  176.3 67.1 %all_to_all.10 = bf16[16,32,2048]{2,1,0:T(8,128)(2,1)S(1)} all-to-all(bf16[16,32,2048]{2,1,0:T(8,128)(2,1)} %bitcast.9), channel_id=1, replica_groups=mesh['grp'=2,'fs'=16,'tp'=16] {'tp'}, dimensions={0} | all-to-all | bytes 4194304 | tf_op jit(solution)/shard_map/all_to_all | solution.py:42
  243.4 0.0 copy-start.1
  243.4 0.0 copy-start.2
  243.4 0.4 convert_reduce_fusion
  243.8 0.3 copy-done.1
  244.1 0.1 multiply_reduce_fusion
  244.3 0.0 copy-done.2
  244.3 0.8 multiply_convert_fusion
  245.0 0.1 all-gather.5.cloned.1.call-update
  245.1 37.2 %all-gather.5.cloned.1.call-done = bf16[512,2048]{1,0:T(8,128)(2,1)} async-done(((bf16[32,2048]{1,0:T(8,128)(2,1)}), bf16[512,2048]{1,0:T(8,128)(2,1)}) %all-gather.5.cloned.1.call-update) | async-done | bytes 2097168 | tf_op jit(solution)/shard_map/all_gather | solution.py:80
  282.3 3.2 %copy.17 = bf16[512,2048]{1,0:T(8,128)(2,1)} copy(bf16[512,2048]{1,0:T(8,128)(2,1)} %all-gather.5.cloned.1.call-done) | data formatting | bytes 4194304
  (2 shorter events, 0.0 us)
Async XLA Ops:
  6.5 161.3 %all-gather.3.cloned.1.call-start = ((), (), s32[]{:S(2)}) async-start(), calls=%async_computation.2 | async-start | bytes 3063808 | tf_op jit(solution)/shard_map/all_gather | solution.py:15
  10.1 45.7 %copy-start = (bf16[512,2048]{1,0:T(8,128)(2,1)S(1)}, bf16[512,2048]{1,0:T(8,128)(2,1)}, u32[]{:S(2)}) copy-start(bf16[512,2048]{1,0:T(8,128)(2,1)} %param.9) | copy-start | bytes 6291460
  11.4 156.4 %copy-start.3 = (f32[2048]{0:T(1024)S(1)}, f32[2048]{0:T(1024)}, u32[]{:S(2)}) copy-start(f32[2048]{0:T(1024)} %param.10) | copy-start | bytes 24580
  11.4 156.4 %copy-start.4 = (f32[352]{0:T(512)S(1)}, f32[352]{0:T(512)}, u32[]{:S(2)}) copy-start(f32[352]{0:T(512)} %param.12) | copy-start | bytes 4228
  11.4 159.7 %all-to-all-start = ((bf16[16,352,128]{2,1,0:T(8,128)(2,1)}), bf16[16,352,128]{2,1,0:T(8,128)(2,1)S(1)}, u32[]{:S(2)}, u32[]{:S(2)}) async-start(bf16[16,352,128]{2,1,0:T(8,128)(2,1)} %broadcast_in_dim.2), calls=%async_computation | async-start | bytes 2883584 | tf_op jit(solution)/shard_map/all_to_all | solution.py:20
  55.8 226.5 %all-gather.5.cloned.1.call-start = ((), (), s32[]{:S(2)}) async-start(), calls=%async_computation.3 | async-start | bytes 2228224 | tf_op jit(solution)/shard_map/all_gather | solution.py:80
  243.4 0.7 copy-start.1
  243.4 0.8 copy-start.2
Sparse Core Ops, SparseCore 0:
  9.4 158.4 all-gather.2
  245.2 37.0 all-gather.4
where the time goes:
time: 293 us; the launch traced here: 292 us
  waiting for transfers between devices  149 us (51%)
  blocking collectives  67.1 us (23%)
  starting transfers between devices  44.4 us (15%)
  between operations  13.5 us (5%)
  matrix products  8.45 us (3%)
  other arithmetic  5.27 us (2%)
  local copies, waits for them, and re-layouts  4.77 us (2%)
    all_gather x1, waiting for transfers between devices, side_by_side(): lax.all_gather(both, axis, axis=dim, tiled=True)  111 us
    all_to_all x1, blocking collectives, sent_and_summed(): parts = lax.all_to_all(cut_along(array, dim, count), axis, 0, 0, tiled=True)  67.1 us
    all_to_all x1, starting transfers between devices, from_everyone(): return lax.all_to_all(copies, axis, split_axis=0, concat_axis=0, tiled=True)  44.4 us
    all_gather x1, waiting for transfers between devices, body(): return lax.all_gather(scaled, 'tp', axis=0, tiled=True)  37.2 us
  transfers between devices with their start and end apart: 3, of which 2 were waited for; matrix products, arithmetic and copies ran while one was open for 2% of the time, Pallas kernels for 0%

commit v1 on v0

--- a/solution.py
+++ b/solution.py
@@ -4,6 +4,12 @@
 from jax.sharding import PartitionSpec as P
 
 EPS = 1e-06
+
+
+def _wait_lanes(my_data, dim_no):
+    my_data = jnp.moveaxis(my_data, 0, dim_no)
+    y_new = my_data.shape
+    return my_data.reshape(*y_new[:dim_no], y_new[dim_no] * y_new[dim_no + 1], *y_new[dim_no + 2 :])
 
 
 def side_by_side(arrays, axis, dim, along):
@@ -61,6 +67,25 @@
     down_scale,
     post_gain,
 ):
+
+    def play_rows(base_x, shard_axis, pos_dim):
+        dev_count = lax.axis_size(shard_axis)
+        column = tuple(((i0, (i0 + 1) % dev_count) for i0 in range(dev_count)))
+        samples = tuple(((w, no) for no, w in column))
+        item_now, q_next = ([], [])
+        for c in range(dev_count - 1):
+            if c % 2 == 0:
+                item_now.append(
+                    lax.ppermute(item_now[-1] if item_now else base_x, shard_axis, perm=column)
+                )
+            else:
+                q_next.append(lax.ppermute(q_next[-1] if q_next else base_x, shard_axis, samples))
+        mid_arr = jnp.stack([*item_now[::-1], base_x, *q_next], axis=0)
+        z = lax.axis_index(shard_axis)
+        seen_now = z - len(item_now)
+        mid_arr = mid_arr[(jnp.arange(dev_count) - seen_now) % dev_count]
+        return _wait_lanes(mid_arr, pos_dim)
+
     rows = tokens.astype(jnp.float32)
     normed = (
         rows * lax.rsqrt(jnp.mean(rows * rows, axis=-1, keepdims=True) + EPS) * pre_gain
@@ -77,7 +102,7 @@
         jnp.dot(hidden, down_full, preferred_element_type=jnp.float32).astype(jnp.bfloat16), "tp", 0
     )
     scaled = finish(summed, down_scale, post_gain)
-    return lax.all_gather(scaled, "tp", axis=0, tiled=True)
+    return play_rows(scaled, "tp", 0)
 
 
 def solution(mesh):

time: 293 us -> 298 us (1.017)
  starting transfers between devices: 44.4 us -> 72.8 us
  waiting for transfers between devices: 149 us -> 121 us
    all_gather x1 -> x0, waiting for transfers between devices: 37.2 us -> none  [body(): return lax.all_gather(scaled, 'tp', axis=0, tiled=True)]
    ppermute x0 -> x15, starting transfers between devices: none -> 28.4 us  [the longest x7 20.1 us: play_rows(): lax.ppermute(q_next[-1] if q_next else base_x, shard_axis, samples)]
    ppermute x0 -> x15, waiting for transfers between devices: none -> 9.39 us  [the longest x8 7.54 us: play_rows(): lax.ppermute(item_now[-1] if item_now else base_x, shard_axis, perm=column)]
  transfers between devices with their start and end apart: 3 -> 17, of which waited for: 2 -> 14; matrix products, arithmetic and copies ran while one was open for 2% -> 3% of each run, Pallas kernels for 0% -> 0%
where the time goes in v1:
time: 298 us; the launch traced here: 294 us
  waiting for transfers between devices  121 us (41%)
  starting transfers between devices  72.8 us (24%)
  blocking collectives  66.5 us (22%)
  between operations  13.7 us (5%)
  matrix products  7.77 us (3%)
  local copies, waits for them, and re-layouts  7.09 us (2%)
  other arithmetic  5.33 us (2%)
    all_gather x1, waiting for transfers between devices, side_by_side(): lax.all_gather(both, axis, axis=dim, tiled=True)  112 us
    all_to_all x1, blocking collectives, sent_and_summed(): parts = lax.all_to_all(cut_along(array, dim, count), axis, 0, 0, tiled=True)  66.5 us
    all_to_all x1, starting transfers between devices, from_everyone(): return lax.all_to_all(copies, axis, split_axis=0, concat_axis=0, tiled=True)  44.4 us
    ppermute x7, starting transfers between devices, play_rows(): lax.ppermute(q_next[-1] if q_next else base_x, shard_axis, samples)  20.1 us
    ppermute x8, starting transfers between devices, play_rows(): lax.ppermute(item_now[-1] if item_now else base_x, shard_axis, perm=column)  8.38 us
    ppermute x8, waiting for transfers between devices, play_rows(): lax.ppermute(item_now[-1] if item_now else base_x, shard_axis, perm=column)  7.54 us
  transfers between devices with their start and end apart: 17, of which 14 were waited for; matrix products, arithmetic and copies ran while one was open for 3% of the time, Pallas kernels for 0%

profile of v1, /device:TPU:65, one launch (start us, length us, event | category | flops | bytes accessed | tf_op | source)
XLA Modules:
  0.0 294.4 jit_solution(11247523801610918864)
XLA Ops:
  6.6 0.9 convert_element_type.38
  7.5 0.9 convert_element_type.39
  8.4 0.7 pad_maximum_fusion
  9.1 0.1 all-gather.2.cloned.1.call-update
  9.2 0.9 convert_element_type.41
  10.1 1.3 broadcast_in_dim.2
  11.4 44.4 %all-to-all-start = ((bf16[16,352,128]{2,1,0:T(8,128)(2,1)}), bf16[16,352,128]{2,1,0:T(8,128)(2,1)}, u32[]{:S(2)}, u32[]{:S(2)}) async-start(bf16[16,352,128]{2,1,0:T(8,128)(2,1)} %broadcast_in_dim.2), calls=%async_computation | async-start | bytes 2883584 | tf_op jit(solution)/shard_map/all_to_all | solution.py:26
  55.8 0.5 fusion
  56.3 111.8 %all-gather.2.cloned.1.call-done = bf16[2048,704]{0,1:T(8,128)(2,1)} async-done(((bf16[128,704]{0,1:T(8,128)(2,1)}), bf16[2048,704]{0,1:T(8,128)(2,1)}) %all-gather.2.cloned.1.call-update) | async-done | bytes 2883600 | tf_op jit(solution)/shard_map/all_gather | solution.py:21
  168.1 2.4 fusion.9
  170.5 5.4 %convolution_convert_fusion = bf16[512,2048]{1,0:T(8,128)(2,1)} fusion(bf16[2048,704]{0,1:T(8,128)(2,1)} %all-gather.2.cloned.1.call-done, f32[512,352]{0,1:T(8,128)S(1)} %fusion.9, bf16[512,2048]{1,0:T(8,128)(2,1)S(1)} %copy-done, f32[2048]{0:T(1024)S(1)} %copy-done.8, f32[512]{0:T(512)S(1)} %add_rsqrt_fusion, f32[352]{0:T(512)S(1)} %copy-done.10, ...), kind=kOutput, calls=%fused_computation.7 | convolution fusion | flops 1482899456 | bytes 7810432 | tf_op jit(solution)/shard_map/dot_general | solution.py:102
  175.9 66.5 %all_to_all.10 = bf16[16,32,2048]{2,1,0:T(8,128)(2,1)S(1)} all-to-all(bf16[16,32,2048]{2,1,0:T(8,128)(2,1)} %bitcast.52), channel_id=1, replica_groups=mesh['grp'=2,'fs'=16,'tp'=16] {'tp'}, dimensions={0} | all-to-all | bytes 4194304 | tf_op jit(solution)/shard_map/all_to_all | solution.py:48
  242.4 0.4 convert_reduce_fusion
  242.8 0.3 copy-done.4
  243.1 0.1 multiply_reduce_fusion
  243.3 0.1 multiply_convert_fusion
  243.4 0.1 collective-permute-start
  243.5 1.9 collective-permute-done
  245.4 2.4 collective-permute-start.1
  247.9 0.0 collective-permute-start.8
  247.9 1.9 collective-permute-done.1
  249.8 2.4 collective-permute-start.2
  252.2 0.3 collective-permute-done.8
  252.5 0.9 collective-permute-start.9
  253.5 0.8 collective-permute-done.2
  254.3 2.3 collective-permute-start.3
  256.6 0.3 collective-permute-done.9
  256.9 2.2 collective-permute-start.10
  259.1 0.8 collective-permute-done.3
  259.9 1.1 collective-permute-start.4
  261.0 0.3 collective-permute-done.10
  261.3 3.4 %collective-permute-start.11 = (bf16[32,2048]{1,0:T(8,128)(2,1)S(1)}, bf16[32,2048]{1,0:T(8,128)(2,1)S(1)}, u32[]{:S(2)}, u32[]{:S(2)}) collective-permute-start(bf16[32,2048]{1,0:T(8,128)(2,1)S(1)} %collective-permute-done.10), channel_id=1, source_target_pairs={{1,0},{2,1},{3,2},{4,3},{5,4},{6,5},{7,6},{8,7},{9,8},{10,9},{11,1... | collective-permute-start | bytes 393224 | tf_op jit(solution)/shard_map/ppermute | solution.py:82
  264.7 0.8 collective-permute-done.4
  265.5 0.2 collective-permute-done.11
  265.7 0.5 copy-done.1
  266.2 4.8 %collective-permute-start.12 = (bf16[32,2048]{1,0:T(8,128)(2,1)S(1)}, bf16[32,2048]{1,0:T(8,128)(2,1)S(1)}, u32[]{:S(2)}, u32[]{:S(2)}) collective-permute-start(bf16[32,2048]{1,0:T(8,128)(2,1)S(1)} %collective-permute-done.11), channel_id=1, source_target_pairs={{1,0},{2,1},{3,2},{4,3},{5,4},{6,5},{7,6},{8,7},{9,8},{10,9},{11,1... | collective-permute-start | bytes 393224 | tf_op jit(solution)/shard_map/ppermute | solution.py:82
  270.9 0.2 collective-permute-done.5
  271.1 0.8 collective-permute-done.12
  271.9 4.0 %collective-permute-start.13 = (bf16[32,2048]{1,0:T(8,128)(2,1)S(1)}, bf16[32,2048]{1,0:T(8,128)(2,1)S(1)}, u32[]{:S(2)}, u32[]{:S(2)}) collective-permute-start(bf16[32,2048]{1,0:T(8,128)(2,1)S(1)} %collective-permute-done.12), channel_id=1, source_target_pairs={{1,0},{2,1},{3,2},{4,3},{5,4},{6,5},{7,6},{8,7},{9,8},{10,9},{11,1... | collective-permute-start | bytes 393224 | tf_op jit(solution)/shard_map/ppermute | solution.py:82
  276.0 0.8 collective-permute-done.6
  276.8 0.6 pad_clamp_fusion
  277.4 4.8 %collective-permute-start.14 = (bf16[32,2048]{1,0:T(8,128)(2,1)S(1)}, bf16[32,2048]{1,0:T(8,128)(2,1)S(1)}, u32[]{:S(2)}, u32[]{:S(2)}) collective-permute-start(bf16[32,2048]{1,0:T(8,128)(2,1)S(1)} %collective-permute-done.13), channel_id=1, source_target_pairs={{1,0},{2,1},{3,2},{4,3},{5,4},{6,5},{7,6},{8,7},{9,8},{10,9},{11,1... | collective-permute-start | bytes 393224 | tf_op jit(solution)/shard_map/ppermute | solution.py:82
  282.1 0.2 collective-permute-done.7
  282.4 0.9 bitcast_dynamic-update-slice_fusion.13
  283.3 0.9 bitcast_dynamic-update-slice_fusion.12
  284.2 0.9 bitcast_dynamic-update-slice_fusion.11
  285.2 0.1 fusion.36
  285.4 2.1 gather_fusion
  (42 shorter events, 0.2 us)
Async XLA Ops:
  6.5 161.6 %all-gather.2.cloned.1.call-start = ((), (), s32[]{:S(2)}) async-start(), calls=%async_computation.2 | async-start | bytes 3063808 | tf_op jit(solution)/shard_map/all_gather | solution.py:21
  10.1 45.7 %copy-start = (bf16[512,2048]{1,0:T(8,128)(2,1)S(1)}, bf16[512,2048]{1,0:T(8,128)(2,1)}, u32[]{:S(2)}) copy-start(bf16[512,2048]{1,0:T(8,128)(2,1)} %param.9) | copy-start | bytes 6291460
  11.4 156.7 %copy-start.8 = (f32[2048]{0:T(1024)S(1)}, f32[2048]{0:T(1024)}, u32[]{:S(2)}) copy-start(f32[2048]{0:T(1024)} %param.10) | copy-start | bytes 24580
  11.4 156.7 %copy-start.9 = (f32[352]{0:T(512)S(1)}, f32[352]{0:T(512)}, u32[]{:S(2)}) copy-start(f32[352]{0:T(512)} %param.12) | copy-start | bytes 4228
  11.4 159.1 %all-to-all-start = ((bf16[16,352,128]{2,1,0:T(8,128)(2,1)}), bf16[16,352,128]{2,1,0:T(8,128)(2,1)}, u32[]{:S(2)}, u32[]{:S(2)}) async-start(bf16[16,352,128]{2,1,0:T(8,128)(2,1)} %broadcast_in_dim.2), calls=%async_computation | async-start | bytes 2883584 | tf_op jit(solution)/shard_map/all_to_all | solution.py:26
  56.3 114.2 %copy-start.10 = (f32[352]{0:T(512)S(1)}, f32[352]{0:T(512)}, u32[]{:S(2)}) copy-start(f32[352]{0:T(512)} %param.14) | copy-start | bytes 4228
  242.4 0.7 copy-start.4
  242.4 0.8 copy-start.5
  243.3 4.6 %copy-start.6 = (f32[32]{0:T(128)}, f32[32]{0:T(128)S(1)}, u32[]{:S(2)}) copy-start(f32[32]{0:T(128)S(1)} %add_rsqrt_fusion.1) | copy-start | bytes 388
  243.4 2.0 collective-permute-start
  245.4 4.4 %collective-permute-start.1 = (bf16[32,2048]{1,0:T(8,128)(2,1)S(1)}, bf16[32,2048]{1,0:T(8,128)(2,1)S(1)}, u32[]{:S(2)}, u32[]{:S(2)}) collective-permute-start(bf16[32,2048]{1,0:T(8,128)(2,1)S(1)} %collective-permute-done), channel_id=1, source_target_pairs={{0,1},{1,2},{2,3},{3,4},{4,5},{5,6},{6,7},{7,8},{8,9},{9,10},{10,1... | collective-permute-start | bytes 393224 | tf_op jit(solution)/shard_map/ppermute | solution.py:79
  247.9 4.7 %collective-permute-start.8 = (bf16[32,2048]{1,0:T(8,128)(2,1)S(1)}, bf16[32,2048]{1,0:T(8,128)(2,1)S(1)}, u32[]{:S(2)}, u32[]{:S(2)}) collective-permute-start(bf16[32,2048]{1,0:T(8,128)(2,1)S(1)} %multiply_convert_fusion), channel_id=1, source_target_pairs={{1,0},{2,1},{3,2},{4,3},{5,4},{6,5},{7,6},{8,7},{9,8},{10,9},{11,1... | collective-permute-start | bytes 393224 | tf_op jit(solution)/shard_map/ppermute | solution.py:82
  249.8 4.5 %collective-permute-start.2 = (bf16[32,2048]{1,0:T(8,128)(2,1)S(1)}, bf16[32,2048]{1,0:T(8,128)(2,1)S(1)}, u32[]{:S(2)}, u32[]{:S(2)}) collective-permute-start(bf16[32,2048]{1,0:T(8,128)(2,1)S(1)} %collective-permute-done.1), channel_id=1, source_target_pairs={{0,1},{1,2},{2,3},{3,4},{4,5},{5,6},{6,7},{7,8},{8,9},{9,10},{10,1... | collective-permute-start | bytes 393224 | tf_op jit(solution)/shard_map/ppermute | solution.py:79
  252.5 4.4 %collective-permute-start.9 = (bf16[32,2048]{1,0:T(8,128)(2,1)S(1)}, bf16[32,2048]{1,0:T(8,128)(2,1)S(1)}, u32[]{:S(2)}, u32[]{:S(2)}) collective-permute-start(bf16[32,2048]{1,0:T(8,128)(2,1)S(1)} %collective-permute-done.8), channel_id=1, source_target_pairs={{1,0},{2,1},{3,2},{4,3},{5,4},{6,5},{7,6},{8,7},{9,8},{10,9},{11,1... | collective-permute-start | bytes 393224 | tf_op jit(solution)/shard_map/ppermute | solution.py:82
  254.3 5.6 %collective-permute-start.3 = (bf16[32,2048]{1,0:T(8,128)(2,1)S(1)}, bf16[32,2048]{1,0:T(8,128)(2,1)S(1)}, u32[]{:S(2)}, u32[]{:S(2)}) collective-permute-start(bf16[32,2048]{1,0:T(8,128)(2,1)S(1)} %collective-permute-done.2), channel_id=1, source_target_pairs={{0,1},{1,2},{2,3},{3,4},{4,5},{5,6},{6,7},{7,8},{8,9},{9,10},{10,1... | collective-permute-start | bytes 393224 | tf_op jit(solution)/shard_map/ppermute | solution.py:79
  256.9 4.4 %collective-permute-start.10 = (bf16[32,2048]{1,0:T(8,128)(2,1)S(1)}, bf16[32,2048]{1,0:T(8,128)(2,1)S(1)}, u32[]{:S(2)}, u32[]{:S(2)}) collective-permute-start(bf16[32,2048]{1,0:T(8,128)(2,1)S(1)} %collective-permute-done.9), channel_id=1, source_target_pairs={{1,0},{2,1},{3,2},{4,3},{5,4},{6,5},{7,6},{8,7},{9,8},{10,9},{11,1... | collective-permute-start | bytes 393224 | tf_op jit(solution)/shard_map/ppermute | solution.py:82
  259.9 5.6 %collective-permute-start.4 = (bf16[32,2048]{1,0:T(8,128)(2,1)S(1)}, bf16[32,2048]{1,0:T(8,128)(2,1)S(1)}, u32[]{:S(2)}, u32[]{:S(2)}) collective-permute-start(bf16[32,2048]{1,0:T(8,128)(2,1)S(1)} %collective-permute-done.3), channel_id=1, source_target_pairs={{0,1},{1,2},{2,3},{3,4},{4,5},{5,6},{6,7},{7,8},{8,9},{9,10},{10,1... | collective-permute-start | bytes 393224 | tf_op jit(solution)/shard_map/ppermute | solution.py:79
  261.3 4.4 %collective-permute-start.11 = (bf16[32,2048]{1,0:T(8,128)(2,1)S(1)}, bf16[32,2048]{1,0:T(8,128)(2,1)S(1)}, u32[]{:S(2)}, u32[]{:S(2)}) collective-permute-start(bf16[32,2048]{1,0:T(8,128)(2,1)S(1)} %collective-permute-done.10), channel_id=1, source_target_pairs={{1,0},{2,1},{3,2},{4,3},{5,4},{6,5},{7,6},{8,7},{9,8},{10,9},{11,1... | collective-permute-start | bytes 393224 | tf_op jit(solution)/shard_map/ppermute | solution.py:82
  265.5 0.6 copy-start.1
  265.5 5.6 %collective-permute-start.5 = (bf16[32,2048]{1,0:T(8,128)(2,1)S(1)}, bf16[32,2048]{1,0:T(8,128)(2,1)S(1)}, u32[]{:S(2)}, u32[]{:S(2)}) collective-permute-start(bf16[32,2048]{1,0:T(8,128)(2,1)S(1)} %collective-permute-done.4), channel_id=1, source_target_pairs={{0,1},{1,2},{2,3},{3,4},{4,5},{5,6},{6,7},{7,8},{8,9},{9,10},{10,1... | collective-permute-start | bytes 393224 | tf_op jit(solution)/shard_map/ppermute | solution.py:79
  266.2 5.7 %collective-permute-start.12 = (bf16[32,2048]{1,0:T(8,128)(2,1)S(1)}, bf16[32,2048]{1,0:T(8,128)(2,1)S(1)}, u32[]{:S(2)}, u32[]{:S(2)}) collective-permute-start(bf16[32,2048]{1,0:T(8,128)(2,1)S(1)} %collective-permute-done.11), channel_id=1, source_target_pairs={{1,0},{2,1},{3,2},{4,3},{5,4},{6,5},{7,6},{8,7},{9,8},{10,9},{11,1... | collective-permute-start | bytes 393224 | tf_op jit(solution)/shard_map/ppermute | solution.py:82
  271.1 11.0 %copy-start.2 = (bf16[32,2048]{1,0:T(8,128)(2,1)}, bf16[32,2048]{1,0:T(8,128)(2,1)S(1)}, u32[]{:S(2)}) copy-start(bf16[32,2048]{1,0:T(8,128)(2,1)S(1)} %collective-permute-done.5) | copy-start | bytes 393220
  271.1 5.6 %collective-permute-start.6 = (bf16[32,2048]{1,0:T(8,128)(2,1)S(1)}, bf16[32,2048]{1,0:T(8,128)(2,1)S(1)}, u32[]{:S(2)}, u32[]{:S(2)}) collective-permute-start(bf16[32,2048]{1,0:T(8,128)(2,1)S(1)} %collective-permute-done.5), channel_id=1, source_target_pairs={{0,1},{1,2},{2,3},{3,4},{4,5},{5,6},{6,7},{7,8},{8,9},{9,10},{10,1... | collective-permute-start | bytes 393224 | tf_op jit(solution)/shard_map/ppermute | solution.py:79
  271.1 14.1 %copy-start.7 = (f32[32]{0:T(128)S(1)}, f32[32]{0:T(128)}, u32[]{:S(2)}) copy-start(f32[32]{0:T(128)} %copy-done.6) | copy-start | bytes 388
  271.9 5.4 %collective-permute-start.13 = (bf16[32,2048]{1,0:T(8,128)(2,1)S(1)}, bf16[32,2048]{1,0:T(8,128)(2,1)S(1)}, u32[]{:S(2)}, u32[]{:S(2)}) collective-permute-start(bf16[32,2048]{1,0:T(8,128)(2,1)S(1)} %collective-permute-done.12), channel_id=1, source_target_pairs={{1,0},{2,1},{3,2},{4,3},{5,4},{6,5},{7,6},{8,7},{9,8},{10,9},{11,1... | collective-permute-start | bytes 393224 | tf_op jit(solution)/shard_map/ppermute | solution.py:82
  276.7 5.4 %copy-start.3 = (bf16[32,2048]{1,0:T(8,128)(2,1)}, bf16[32,2048]{1,0:T(8,128)(2,1)S(1)}, u32[]{:S(2)}) copy-start(bf16[32,2048]{1,0:T(8,128)(2,1)S(1)} %collective-permute-done.6) | copy-start | bytes 393220
  276.7 5.6 %collective-permute-start.7 = (bf16[32,2048]{1,0:T(8,128)(2,1)S(1)}, bf16[32,2048]{1,0:T(8,128)(2,1)S(1)}, u32[]{:S(2)}, u32[]{:S(2)}) collective-permute-start(bf16[32,2048]{1,0:T(8,128)(2,1)S(1)} %collective-permute-done.6), channel_id=1, source_target_pairs={{0,1},{1,2},{2,3},{3,4},{4,5},{5,6},{6,7},{7,8},{8,9},{9,10},{10,1... | collective-permute-start | bytes 393224 | tf_op jit(solution)/shard_map/ppermute | solution.py:79
  277.4 8.0 %collective-permute-start.14 = (bf16[32,2048]{1,0:T(8,128)(2,1)S(1)}, bf16[32,2048]{1,0:T(8,128)(2,1)S(1)}, u32[]{:S(2)}, u32[]{:S(2)}) collective-permute-start(bf16[32,2048]{1,0:T(8,128)(2,1)S(1)} %collective-permute-done.13), channel_id=1, source_target_pairs={{1,0},{2,1},{3,2},{4,3},{5,4},{6,5},{7,6},{8,7},{9,8},{10,9},{11,1... | collective-permute-start | bytes 393224 | tf_op jit(solution)/shard_map/ppermute | solution.py:82
Sparse Core Ops, SparseCore 0:
  9.4 158.6 all-gather.1
